TPU v7x, 512 devices: a whole 4x4x16 slice. The times are simulated.
512 devices in a mesh: sp: 16 (over z), fs: 4 (over y), tp: 8 (over x, core).
Axes of the slice: x: 4, y: 4, z: 16, core: 2. Of those that a mesh axis runs over, the one named last changes fastest.
Arguments:
- inputs: bfloat16 [4, 4096, 4096], P('fs', 'sp', 'tp'), may hold values from -6 to 6
- norm_gain: float32 [4096], replicated, may hold values from 0.1 to 1.9
- conv_in_a: bfloat16 [4096, 1024], P(('sp', 'fs'), 'tp'), may hold values from -0.09375 to 0.09375
- conv_in_b: bfloat16 [4096, 1024], P(('sp', 'fs'), 'tp'), may hold values from -0.09375 to 0.09375
- query_w: bfloat16 [4096, 512], P(('sp', 'fs'), 'tp'), may hold values from -0.09375 to 0.09375
- key_w: bfloat16 [4096, 512], P(('sp', 'fs'), 'tp'), may hold values from -0.09375 to 0.09375
- value_w: bfloat16 [4096, 1024], P(('sp', 'fs'), 'tp'), may hold values from -0.09375 to 0.09375
- out_gate_w: bfloat16 [4096, 1024], P(('sp', 'fs'), 'tp'), may hold values from -0.09375 to 0.09375
- pointwise_w: bfloat16 [4096, 1024], P(('sp', 'fs'), 'tp'), may hold values from -0.1875 to 0.1875
- gla_out_w: bfloat16 [4096, 1024], P(('sp', 'fs'), 'tp'), may hold values from -0.1875 to 0.1875
- forget_first_factor: bfloat16 [4096, 64], replicated, may hold values from -0.09375 to 0.09375
- decay_w: bfloat16 [64, 512], replicated, may hold values from -0.75 to 0.75
- decay_bias: float32 [512], replicated, as said below
- decay_extra: float32 [4, 4096, 512], P('fs', 'sp', 'tp'), may hold values from -2.2 to 0, as said below
- conv_kernel: float32 [31, 1024], replicated, may hold values from -7 to 7
- conv_gain: float32 [1024], replicated, may hold values from 0.1 to 1.9
- head_gain: float32 [64], replicated, may hold values from 0.1 to 1.9
Outputs:
- mixed: bfloat16 [4, 4096, 4096], P('fs', 'sp', 'tp')
Inputs may be any that keep to these rules, and one draw needn't show every extreme that they name: decay_bias is positive. decay_extra is never positive.
All inputs are finite; a program needn't handle non-finite values.
Results may differ from a plain program's by a relative error of at most 0.015.
Values may be sent and summed in bfloat16 or wider, within the bound.
A program may use at most 128 MiB of HBM per device.

v0:
```python
import jax
import jax.numpy as jnp
from jax import lax
from jax.sharding import PartitionSpec as P

DK = 32
DV = 64
BLOCK = 64


def side_by_side(arrays, axis, dim, along):
    ends, at = ([], 0)
    for a in arrays[:-1]:
        at += a.shape[along]
        ends.append(at)
    both = jnp.concatenate(arrays, axis=along)
    return tuple(jnp.split(lax.all_gather(both, axis, axis=dim, tiled=True), ends, axis=along))


def from_everyone(value, axis):
    length = lax.axis_size(axis)
    return lax.all_to_all(
        jnp.broadcast_to(value[None], (length, *value.shape)), axis, 0, 0, tiled=True
    )


def in_order(tiles, dim):
    lengths = list(tiles.shape[1:])
    lengths[dim] *= tiles.shape[0]
    return jnp.moveaxis(tiles, 0, dim).reshape(lengths)


def gathered_copies(value, axis, dim):
    tiles = from_everyone(value, axis)
    return in_order(tiles, dim)


def from_behind(value, axis, by):
    length = lax.axis_size(axis)
    pairs = [(i, i + by) for i in range(length) if 0 <= i + by < length]
    return lax.ppermute(value, axis, pairs)


def over_copies(value, axis):
    everything = from_everyone(value, axis)
    return jnp.sum(everything, axis=0)


def in_one(arrays, axis):
    vector, at, outs = (jnp.concatenate([a.reshape(-1) for a in arrays]), 0, [])
    subtotal = over_copies(vector, axis)
    for a in arrays:
        outs.append(subtotal[at : at + a.size].reshape(a.shape))
        at += a.size
    return tuple(outs)


def in_blocks(value, dim, length):
    lengths = value.shape
    tiles = value.reshape(*lengths[:dim], length, lengths[dim] // length, *lengths[dim + 1 :])
    return jnp.moveaxis(tiles, dim, 0)


def sum_at_owner(value, axis, dim):
    length = lax.axis_size(axis)
    tiles = lax.all_to_all(in_blocks(value, dim, length), axis, 0, 0, tiled=True)
    return jnp.sum(tiles.astype(jnp.float32), axis=0)


def shards(
    inputs,
    norm_gain,
    conv_in_a,
    conv_in_b,
    query_w,
    key_w,
    value_w,
    out_gate_w,
    pointwise_w,
    gla_out_w,
    forget_first_factor,
    decay_w,
    decay_bias,
    decay_extra,
    conv_kernel,
    conv_gain,
    head_gain,
):
    nearer = side_by_side(
        (conv_in_a, conv_in_b, query_w, key_w, value_w, out_gate_w, pointwise_w, gla_out_w),
        "fs",
        0,
        1,
    )
    collected = side_by_side(
        (nearer[0], nearer[1], nearer[2], nearer[3], nearer[4], nearer[5], nearer[6], nearer[7]),
        "sp",
        0,
        1,
    )
    (
        conv_a_full,
        conv_b_full,
        query_full,
        key_full,
        value_full,
        gate_full,
        pointwise_full,
        gla_out_full,
    ) = collected
    tok_rows = inputs[0]
    token_count = tok_rows.shape[0]
    in_weights = (
        conv_a_full,
        conv_b_full,
        query_full,
        key_full,
        value_full,
        gate_full,
        forget_first_factor,
    )
    segment_values = gathered_copies(tok_rows, "tp", 1).astype(jnp.float32)
    scaled = (segment_values * norm_gain).astype(jnp.bfloat16)
    sums = tuple(
        (jnp.dot(scaled, weight, preferred_element_type=jnp.float32) for weight in in_weights)
    )
    sums, squares = (sums, jnp.sum(segment_values * segment_values, axis=1))
    row_scale = lax.rsqrt(squares / norm_gain.shape[0] + 1e-06)[:, None]
    conv_a, conv_b, queries, keys, values, out_gate, low_rank = [
        (running * row_scale).astype(jnp.bfloat16) for running in sums
    ]
    gated = (conv_a.astype(jnp.float32) * jax.nn.sigmoid(conv_b.astype(jnp.float32))).astype(
        jnp.bfloat16
    )
    reach = conv_kernel.shape[0] - 1
    earlier = from_behind(gated[token_count - reach :], "sp", 1)
    extended = jnp.concatenate([earlier, gated], axis=0).astype(jnp.float32)
    tp_index = lax.axis_index("tp")
    channels = gated.shape[1]
    kernel = lax.dynamic_slice_in_dim(conv_kernel, tp_index * channels, channels, 1)
    convolved = jnp.zeros((token_count, channels), jnp.float32)
    for offset in range(reach + 1):
        convolved = convolved + kernel[offset] * extended[offset : offset + token_count]
    channel_sum, channel_squares = in_one(
        (jnp.sum(convolved, axis=1), jnp.sum(convolved * convolved, axis=1)), "tp"
    )
    total_channels = conv_gain.shape[0]
    average = channel_sum / total_channels
    spread_squared_mean = channel_squares / total_channels - average * average
    gain_part = lax.dynamic_slice_in_dim(conv_gain, tp_index * channels, channels)
    normed = (
        (convolved - average[:, None]) * lax.rsqrt(spread_squared_mean + 1e-05)[:, None] * gain_part
    )
    conv_act = jax.nn.silu(normed).astype(jnp.bfloat16)
    key_width = keys.shape[1]
    head_count = key_width // DK
    decay_part = lax.dynamic_slice_in_dim(decay_w, tp_index * key_width, key_width, 1)
    bias_part = lax.dynamic_slice_in_dim(decay_bias, tp_index * key_width, key_width)
    pre_decay = jnp.dot(low_rank, decay_part, preferred_element_type=jnp.float32) + bias_part
    log_decay = jax.nn.log_sigmoid(pre_decay) / 16.0 + decay_extra[0]
    block_count = token_count // BLOCK
    highest = lax.Precision.HIGHEST

    def split_blocks(array_operand, width):
        return array_operand.reshape(block_count, BLOCK, head_count, width).transpose(0, 2, 1, 3)

    q_blocks = split_blocks(queries.astype(jnp.float32), DK) * DK ** (-0.5)
    k_blocks = split_blocks(keys.astype(jnp.float32), DK)
    v_blocks = split_blocks(values.astype(jnp.float32), DV)
    prefix_running_sum = jnp.cumsum(split_blocks(log_decay, DK), axis=2)
    causal = jnp.tril(jnp.ones((BLOCK, BLOCK), dtype=bool))
    spread = prefix_running_sum[:, :, :, None, :] - prefix_running_sum[:, :, None, :, :]
    weights_in = jnp.exp(jnp.where(causal[:, :, None], spread, -jnp.inf))
    scores = jnp.einsum("nhid,nhjd,nhijd->nhij", q_blocks, k_blocks, weights_in, precision=highest)
    inner = jnp.einsum("nhij,nhjv->nhiv", scores, v_blocks, precision=highest)
    block_total = prefix_running_sum[:, :, -1]
    block_state = jnp.einsum(
        "nhjd,nhjv->nhdv",
        k_blocks * jnp.exp(block_total[:, :, None] - prefix_running_sum),
        v_blocks,
        precision=highest,
    )

    def advance(state, block_pair):
        decay_row, added_share_term = block_pair
        return (jnp.exp(decay_row)[..., None] * state + added_share_term, state)

    local_final, local_entering = lax.scan(
        advance, jnp.zeros((head_count, DK, DV), jnp.float32), (block_total, block_state)
    )
    device_total = jnp.sum(block_total, axis=0)
    totals = lax.all_gather(device_total[None], "sp", axis=0, tiled=True)
    running_totals = jnp.cumsum(totals, axis=0)
    sp_index = lax.axis_index("sp")
    before = lax.dynamic_index_in_dim(
        running_totals, sp_index, 0, False
    ) - lax.dynamic_index_in_dim(totals, sp_index, 0, False)
    piece = lax.all_gather(local_final[None], "sp", axis=0, tiled=True)
    number = piece.shape[0]
    anchor = jnp.arange(number, dtype=jnp.int32)
    exponent = jnp.where(
        (anchor < sp_index)[:, None, None], before[None] - running_totals, -jnp.inf
    )
    entering = jnp.einsum("nhd,nhdv->hdv", jnp.exp(exponent), piece, precision=highest)
    passed = jnp.exp(jnp.cumsum(block_total, axis=0) - block_total)
    entering_blocks = passed[..., None] * entering[None] + local_entering
    outer = jnp.einsum(
        "nhid,nhdv->nhiv",
        q_blocks * jnp.exp(prefix_running_sum),
        entering_blocks,
        precision=highest,
    )
    head_output = inner + outer
    normed_heads = (
        head_output
        * lax.rsqrt(jnp.mean(head_output * head_output, axis=-1, keepdims=True) + 1e-06)
        * head_gain
    )
    gla_rows = normed_heads.transpose(0, 2, 1, 3).reshape(token_count, head_count * DV)
    gla_act = (gla_rows * jax.nn.silu(out_gate.astype(jnp.float32))).astype(jnp.bfloat16)
    contract = (((1,), (1,)), ((), ()))
    conv_term = lax.dot_general(
        pointwise_full, conv_act, contract, preferred_element_type=jnp.float32
    )
    summed = sum_at_owner(
        (
            conv_term
            + lax.dot_general(gla_out_full, gla_act, contract, preferred_element_type=jnp.float32)
        ).astype(jnp.bfloat16),
        "tp",
        0,
    )
    return (tok_rows.astype(jnp.float32) + summed.T).astype(jnp.bfloat16)[None]


def solution(mesh):
    return jax.shard_map(
        shards,
        mesh=mesh,
        in_specs=(
            P("fs", "sp", "tp"),
            P(),
            P(("sp", "fs"), "tp"),
            P(("sp", "fs"), "tp"),
            P(("sp", "fs"), "tp"),
            P(("sp", "fs"), "tp"),
            P(("sp", "fs"), "tp"),
            P(("sp", "fs"), "tp"),
            P(("sp", "fs"), "tp"),
            P(("sp", "fs"), "tp"),
            P(),
            P(),
            P(),
            P("fs", "sp", "tp"),
            P(),
            P(),
            P(),
        ),
        out_specs=P("fs", "sp", "tp"),
        check_vma=False,
    )
```

profile of v0, /device:TPU:1, one launch (start us, length us, event | category | flops | bytes accessed | tf_op | source)
XLA Modules:
  0.0 245.8 jit_solution(409942196637541957)
XLA Ops:
  6.5 1.0 concatenate.11
  7.5 12.3 %all_gather.12 = bf16[256,896]{1,0:T(8,128)(2,1)} all-gather(bf16[64,896]{1,0:T(8,128)(2,1)S(1)} %concatenate.11), channel_id=1, replica_groups=mesh['sp'=16,'fs'=4,'tp'=8] {'fs'}, dimensions={0}, use_global_device_ids=true | all-gather | bytes 573440 | tf_op jit(solution)/shard_map/all_gather | solution.py:17
  19.8 1.1 copy.64
  20.9 1.5 broadcast_in_dim.45
  22.4 11.6 %all-to-all-start = ((bf16[8,256,512]{1,2,0:T(8,128)(2,1)}), bf16[8,256,512]{1,2,0:T(8,128)(2,1)S(1)}, u32[]{:S(2)}, u32[]{:S(2)}) async-start(bf16[8,256,512]{1,2,0:T(8,128)(2,1)} %broadcast_in_dim.45), calls=%async_computation | async-start | bytes 4194304 | tf_op jit(solution)/shard_map/all_to_all | solution.py:22
  34.0 0.8 dynamic_slice.30
  34.8 1.3 dynamic_slice.28
  36.1 1.7 dynamic-slice_bitcast_fusion.29
  37.8 1.9 fusion.98
  39.7 20.6 %all-to-all-done = bf16[8,256,512]{1,2,0:T(8,128)(2,1)S(1)} async-done(((bf16[8,256,512]{1,2,0:T(8,128)(2,1)}), bf16[8,256,512]{1,2,0:T(8,128)(2,1)S(1)}, u32[]{:S(2)}, u32[]{:S(2)}) %all-to-all-start) | async-done | bytes 2097184 | tf_op jit(solution)/shard_map/all_to_all | solution.py:22
  60.9 1.8 fusion.2
  62.6 2.2 fusion.86
  65.5 28.2 %all-gather.2 = f32[16,2,32]{2,1,0:T(2,128)S(1)} all-gather(f32[1,2,32]{2,1,0:T(2,128)S(1)} %bitcast.160), channel_id=2, replica_groups=mesh['sp'=16,'fs'=4,'tp'=8] {'sp'}, dimensions={0}, use_global_device_ids=true | all-gather | bytes 4352 | tf_op jit(solution)/shard_map/all_gather | solution.py:192
  94.0 4.6 %select_exponential_fusion = f32[4,2,64,64,32]{3,4,2,1,0:T(8,128)} fusion(f32[4,2,64,32]{2,3,1,0:T(8,128)S(1)} %copy.67, f32[4,2,64,32]{3,2,1,0:T(8,128)S(1)} %reduce_window_sum.35, pred[64,64]{1,0:T(8,128)(4,1)S(1)} %iota_compare_fusion), kind=kLoop, calls=%fused_computation.5 | loop fusion | flops 2097152 | bytes 4329472 | tf_op jit(solution)/shard_map/exp | solution.py:173
  98.5 11.0 %copy.82 = f32[4,2,64,64,32]{2,3,4,1,0:T(8,128)} copy(f32[4,2,64,64,32]{3,4,2,1,0:T(8,128)} %select_exponential_fusion) | data formatting | bytes 8388608
  109.6 12.5 %all-gather.5.cloned.1.call-done = bf16[4096,896]{1,0:T(8,128)(2,1)} async-done(((bf16[256,896]{1,0:T(8,128)(2,1)}), bf16[4096,896]{1,0:T(8,128)(2,1)}) %all-gather.5.cloned.1.call-update) | async-done | bytes 7340048 | tf_op jit(solution)/shard_map/all_gather | solution.py:17
  122.1 2.2 fusion.18
  124.4 0.8 copy.73
  125.3 2.0 fusion.13
  127.4 2.0 fusion.38
  129.4 5.8 %while.13 = (s32[]{:T(128)}, f32[2,32,64]{2,1,0:T(8,128)S(1)}, f32[4,2,32,64]{3,2,1,0:T(8,128)}, f32[4,2,32]{2,1,0:T(2,128)S(1)}, f32[4,2,32,64]{3,2,1,0:T(8,128)}, /*index=5*/s32[]{:T(128)}, s32[]{:T(128)}) while((s32[]{:T(128)}, f32[2,32,64]{2,1,0:T(8,128)S(1)}, f32[4,2,32,64]{3,2,1,0:T(8,128)}, f32[4,2,32]{2,1,0:T(2,128)S(1)}, ...), condition=%wide.region_9.10_spmd.clone, body=%wide.region_8.9_spmd.clone.sunk | while | flops 16387 | bytes 99680 | solution.py:188
  129.4 0.6 bitcast_dynamic-update-slice_fusion.2
  130.0 0.8 bitcast_add_fusion.3
  130.8 0.6 bitcast_dynamic-update-slice_fusion.2
  131.4 0.8 bitcast_add_fusion.3
  132.3 0.6 bitcast_dynamic-update-slice_fusion.2
  132.9 0.8 bitcast_add_fusion.3
  133.7 0.6 bitcast_dynamic-update-slice_fusion.2
  134.3 0.8 bitcast_add_fusion.3
  135.2 25.9 %all-gather.1 = f32[32,32,64]{2,1,0:T(8,128)} all-gather(f32[2,32,64]{2,1,0:T(8,128)S(1)} %get-tuple-element.33), channel_id=3, replica_groups=mesh['sp'=16,'fs'=4,'tp'=8] {'sp'}, dimensions={0}, use_global_device_ids=true | all-gather | bytes 278528 | tf_op jit(solution)/shard_map/all_gather | solution.py:198
  161.1 0.7 copy.68
  161.7 1.8 fusion.21
  163.6 0.8 copy.72
  164.5 5.3 %fusion = f32[4,2,64,64]{2,3,1,0:T(8,128)S(1)} fusion(f32[4,2,64,64,32]{2,3,4,1,0:T(8,128)} %copy.82, f32[4,2,32,64]{3,2,1,0:T(8,128)S(1)} %copy.69, f32[4,2,32,64]{3,2,1,0:T(8,128)} %copy.68), kind=kLoop, calls=%fused_computation.4 | loop fusion | flops 3112960 | bytes 4456448 | tf_op jit(solution)/shard_map/nhid,nhjd,nhijd->nhij/dot_general | solution.py:174
  170.4 2.0 fusion.12
  172.4 2.0 fusion.6
  174.4 2.2 collective-permute-start
  176.7 0.9 fusion.34
  177.6 0.8 multiply_reduce_fusion.1
  178.7 1.2 fusion.101
  179.8 0.6 broadcast_in_dim.46
  180.4 12.4 %all-to-all-start.1 = ((f32[8,1,512]{2,1,0:T(1,128)}), f32[8,1,512]{2,1,0:T(1,128)S(1)}, u32[]{:S(2)}, u32[]{:S(2)}) async-start(f32[8,1,512]{2,1,0:T(1,128)} %broadcast_in_dim.46), calls=%async_computation.1 | async-start | bytes 32768 | tf_op jit(solution)/shard_map/all_to_all | solution.py:22
  192.9 0.7 fusion.37
  194.0 3.6 %all-to-all-done.1 = f32[8,1,512]{2,1,0:T(1,128)S(1)} async-done(((f32[8,1,512]{2,1,0:T(1,128)}), f32[8,1,512]{2,1,0:T(1,128)S(1)}, u32[]{:S(2)}, u32[]{:S(2)}) %all-to-all-start.1) | async-done | bytes 16416 | tf_op jit(solution)/shard_map/all_to_all | solution.py:22
  197.6 4.1 %fusion.31 = f32[4096,256]{1,0:T(8,128)} fusion(bf16[4096,896]{1,0:T(8,128)(2,1)} %all-gather.5.cloned.1.call-done, f32[256,128]{1,0:T(8,128)} %get-tuple-element.65, f32[128]{0:T(128)} %dynamic_slice.28, f32[256]{0:T(256)S(1)} %get-tuple-element.100, f32[256]{0:T(256)S(1)} %get-tuple-element.99), kind=kOutput, calls=%fused_computation.50 | convolution fusion | flops 268697600 | bytes 5376512 | tf_op jit(solution)/shard_map/dot_general | solution.py:222
  201.7 5.7 %fusion.1 = bf16[4096,256]{1,0:T(8,128)(2,1)} fusion(f32[4096,256]{1,0:T(8,128)} %fusion.31, bf16[4096,896]{1,0:T(8,128)(2,1)} %all-gather.5.cloned.1.call-done, f32[256,128]{1,0:T(8,128)S(1)} %reshape.78, bf16[256,4096]{0,1:T(8,128)(2,1)S(1)} %copy-done.1, f32[256]{0:T(256)S(1)} %add_rsqrt_fusion.1), kind=kOutput, calls=%fused_computation.7 | convolution fusion | flops 539262976 | bytes 10617856 | tf_op jit(solution)/shard_map/dot_general | solution.py:228
  207.3 30.4 %all_to_all.16 = bf16[8,512,256]{2,1,0:T(8,128)(2,1)S(1)} all-to-all(bf16[8,512,256]{2,1,0:T(8,128)(2,1)} %bitcast.150), channel_id=1, replica_groups=mesh['sp'=16,'fs'=4,'tp'=8] {'tp'}, dimensions={0} | all-to-all | bytes 4194304 | tf_op jit(solution)/shard_map/all_to_all | solution.py:66
  238.1 0.8 copy.77
  (112 shorter events, 3.1 us)
Async XLA Ops:
  6.5 56.1 %copy-start = (bf16[4096,64]{0,1:T(8,128)(2,1)S(1)}, bf16[4096,64]{0,1:T(8,128)(2,1)}, u32[]{:S(2)}) copy-start(bf16[4096,64]{0,1:T(8,128)(2,1)} %param.29) | copy-start | bytes 1572868
  6.5 115.5 %all-gather.5.cloned.1.call-start = ((), (), s32[]{:S(2)}) async-start(), calls=%async_computation.3 | async-start | bytes 7798784 | tf_op jit(solution)/shard_map/all_gather | solution.py:17
  20.9 39.9 %copy-start.6 = (f32[4096]{0:T(1024)S(1)}, f32[4096]{0:T(1024)}, u32[]{:S(2)}) copy-start(f32[4096]{0:T(1024)} %param.20) | copy-start | bytes 49156
  22.4 37.8 %all-to-all-start = ((bf16[8,256,512]{1,2,0:T(8,128)(2,1)}), bf16[8,256,512]{1,2,0:T(8,128)(2,1)S(1)}, u32[]{:S(2)}, u32[]{:S(2)}) async-start(bf16[8,256,512]{1,2,0:T(8,128)(2,1)} %broadcast_in_dim.45), calls=%async_computation | async-start | bytes 4194304 | tf_op jit(solution)/shard_map/all_to_all | solution.py:22
  34.0 28.6 %copy-start.5 = (f32[1,256,64]{1,2,0:T(8,128)S(1)}, f32[1,256,64]{1,2,0:T(8,128)}, u32[]{:S(2)}) copy-start(f32[1,256,64]{1,2,0:T(8,128)} %param.32) | copy-start | bytes 196612
  98.5 23.5 %copy-start.1 = (bf16[256,4096]{0,1:T(8,128)(2,1)S(1)}, bf16[256,4096]{0,1:T(8,128)(2,1)}, u32[]{:S(2)}) copy-start(bf16[256,4096]{0,1:T(8,128)(2,1)} %fusion.2) | copy-start | bytes 6291460
  169.8 6.9 %copy-start.2 = (f32[32,32,64]{2,1,0:T(8,128)S(1)}, f32[32,32,64]{2,1,0:T(8,128)}, u32[]{:S(2)}) copy-start(f32[32,32,64]{2,1,0:T(8,128)} %all-gather.1) | copy-start | bytes 786436
  170.1 7.4 %copy-start.3 = (f32[4,64,2,32]{3,1,2,0:T(8,128)S(1)}, f32[4,64,2,32]{3,1,2,0:T(8,128)}, u32[]{:S(2)}) copy-start(f32[4,64,2,32]{3,1,2,0:T(8,128)} %copy.72) | copy-start | bytes 196612
  170.1 7.4 %copy-start.4 = (f32[4,2,32,64]{3,2,1,0:T(8,128)S(1)}, f32[4,2,32,64]{3,2,1,0:T(8,128)}, u32[]{:S(2)}) copy-start(f32[4,2,32,64]{3,2,1,0:T(8,128)} %get-tuple-element.34) | copy-start | bytes 196612
  170.1 8.2 %copy-start.7 = (f32[128]{0:T(128)S(1)}, f32[128]{0:T(128)}, u32[]{:S(2)}) copy-start(f32[128]{0:T(128)} %get-tuple-element.69) | copy-start | bytes 1540
  170.1 8.2 %copy-start.8 = (f32[128]{0:T(128)S(1)}, f32[128]{0:T(128)}, u32[]{:S(2)}) copy-start(f32[128]{0:T(128)} %get-tuple-element.70) | copy-start | bytes 1540
  170.1 8.2 %copy-start.9 = (f32[128]{0:T(128)S(1)}, f32[128]{0:T(128)}, u32[]{:S(2)}) copy-start(f32[128]{0:T(128)} %get-tuple-element.71) | copy-start | bytes 1540
  170.2 8.2 %copy-start.10 = (f32[128]{0:T(128)S(1)}, f32[128]{0:T(128)}, u32[]{:S(2)}) copy-start(f32[128]{0:T(128)} %get-tuple-element.72) | copy-start | bytes 1540
  170.2 8.2 %copy-start.11 = (f32[128]{0:T(128)S(1)}, f32[128]{0:T(128)}, u32[]{:S(2)}) copy-start(f32[128]{0:T(128)} %get-tuple-element.73) | copy-start | bytes 1540
  170.2 8.2 %copy-start.12 = (f32[128]{0:T(128)S(1)}, f32[128]{0:T(128)}, u32[]{:S(2)}) copy-start(f32[128]{0:T(128)} %get-tuple-element.74) | copy-start | bytes 1540
  170.2 8.2 %copy-start.13 = (f32[128]{0:T(128)S(1)}, f32[128]{0:T(128)}, u32[]{:S(2)}) copy-start(f32[128]{0:T(128)} %get-tuple-element.75) | copy-start | bytes 1540
  170.2 8.2 %copy-start.14 = (f32[128]{0:T(128)S(1)}, f32[128]{0:T(128)}, u32[]{:S(2)}) copy-start(f32[128]{0:T(128)} %get-tuple-element.76) | copy-start | bytes 1540
  170.2 8.2 %copy-start.15 = (f32[128]{0:T(128)S(1)}, f32[128]{0:T(128)}, u32[]{:S(2)}) copy-start(f32[128]{0:T(128)} %get-tuple-element.77) | copy-start | bytes 1540
  170.2 8.2 %copy-start.16 = (f32[128]{0:T(128)S(1)}, f32[128]{0:T(128)}, u32[]{:S(2)}) copy-start(f32[128]{0:T(128)} %get-tuple-element.78) | copy-start | bytes 1540
  170.2 8.2 %copy-start.17 = (f32[128]{0:T(128)S(1)}, f32[128]{0:T(128)}, u32[]{:S(2)}) copy-start(f32[128]{0:T(128)} %get-tuple-element.79) | copy-start | bytes 1540
  170.2 8.2 %copy-start.18 = (f32[128]{0:T(128)S(1)}, f32[128]{0:T(128)}, u32[]{:S(2)}) copy-start(f32[128]{0:T(128)} %get-tuple-element.80) | copy-start | bytes 1540
  170.2 8.2 %copy-start.19 = (f32[128]{0:T(128)S(1)}, f32[128]{0:T(128)}, u32[]{:S(2)}) copy-start(f32[128]{0:T(128)} %get-tuple-element.81) | copy-start | bytes 1540
  170.3 8.2 %copy-start.20 = (f32[128]{0:T(128)S(1)}, f32[128]{0:T(128)}, u32[]{:S(2)}) copy-start(f32[128]{0:T(128)} %get-tuple-element.82) | copy-start | bytes 1540
  170.3 8.2 %copy-start.21 = (f32[128]{0:T(128)S(1)}, f32[128]{0:T(128)}, u32[]{:S(2)}) copy-start(f32[128]{0:T(128)} %get-tuple-element.83) | copy-start | bytes 1540
  170.3 8.2 %copy-start.22 = (f32[128]{0:T(128)S(1)}, f32[128]{0:T(128)}, u32[]{:S(2)}) copy-start(f32[128]{0:T(128)} %get-tuple-element.84) | copy-start | bytes 1540
  170.3 8.2 %copy-start.23 = (f32[128]{0:T(128)S(1)}, f32[128]{0:T(128)}, u32[]{:S(2)}) copy-start(f32[128]{0:T(128)} %get-tuple-element.85) | copy-start | bytes 1540
  170.3 8.2 %copy-start.24 = (f32[128]{0:T(128)S(1)}, f32[128]{0:T(128)}, u32[]{:S(2)}) copy-start(f32[128]{0:T(128)} %get-tuple-element.86) | copy-start | bytes 1540
  170.3 8.2 %copy-start.25 = (f32[128]{0:T(128)S(1)}, f32[128]{0:T(128)}, u32[]{:S(2)}) copy-start(f32[128]{0:T(128)} %get-tuple-element.87) | copy-start | bytes 1540
  170.3 8.2 %copy-start.26 = (f32[128]{0:T(128)S(1)}, f32[128]{0:T(128)}, u32[]{:S(2)}) copy-start(f32[128]{0:T(128)} %get-tuple-element.88) | copy-start | bytes 1540
  170.3 8.2 %copy-start.27 = (f32[128]{0:T(128)S(1)}, f32[128]{0:T(128)}, u32[]{:S(2)}) copy-start(f32[128]{0:T(128)} %get-tuple-element.89) | copy-start | bytes 1540
  170.3 8.2 %copy-start.28 = (f32[128]{0:T(128)S(1)}, f32[128]{0:T(128)}, u32[]{:S(2)}) copy-start(f32[128]{0:T(128)} %get-tuple-element.90) | copy-start | bytes 1540
  170.3 8.2 %copy-start.29 = (f32[128]{0:T(128)S(1)}, f32[128]{0:T(128)}, u32[]{:S(2)}) copy-start(f32[128]{0:T(128)} %get-tuple-element.91) | copy-start | bytes 1540
  170.4 8.2 %copy-start.30 = (f32[128]{0:T(128)S(1)}, f32[128]{0:T(128)}, u32[]{:S(2)}) copy-start(f32[128]{0:T(128)} %get-tuple-element.92) | copy-start | bytes 1540
  170.4 8.2 %copy-start.31 = (f32[128]{0:T(128)S(1)}, f32[128]{0:T(128)}, u32[]{:S(2)}) copy-start(f32[128]{0:T(128)} %get-tuple-element.93) | copy-start | bytes 1540
  170.4 8.2 %copy-start.32 = (f32[128]{0:T(128)S(1)}, f32[128]{0:T(128)}, u32[]{:S(2)}) copy-start(f32[128]{0:T(128)} %get-tuple-element.94) | copy-start | bytes 1540
  170.4 8.2 %copy-start.33 = (f32[128]{0:T(128)S(1)}, f32[128]{0:T(128)}, u32[]{:S(2)}) copy-start(f32[128]{0:T(128)} %get-tuple-element.95) | copy-start | bytes 1540
  170.4 8.2 %copy-start.34 = (f32[128]{0:T(128)S(1)}, f32[128]{0:T(128)}, u32[]{:S(2)}) copy-start(f32[128]{0:T(128)} %get-tuple-element.96) | copy-start | bytes 1540
  170.4 8.2 %copy-start.35 = (f32[128]{0:T(128)S(1)}, f32[128]{0:T(128)}, u32[]{:S(2)}) copy-start(f32[128]{0:T(128)} %get-tuple-element.97) | copy-start | bytes 1540
  170.4 8.2 %copy-start.36 = (f32[128]{0:T(128)S(1)}, f32[128]{0:T(128)}, u32[]{:S(2)}) copy-start(f32[128]{0:T(128)} %get-tuple-element.98) | copy-start | bytes 1540
  174.4 3.9 %collective-permute-start = (bf16[30,128]{1,0:T(8,128)(2,1)S(1)}, bf16[30,128]{1,0:T(8,128)(2,1)S(1)}, u32[]{:S(2)}, u32[]{:S(2)}) collective-permute-start(bf16[30,128]{1,0:T(8,128)(2,1)S(1)} %slice.265), channel_id=1, source_target_pairs={{0,32},{32,64},{64,96},{96,128},{128,160},{160,192},{192,224},{224... | collective-permute-start | bytes 23048 | tf_op jit(solution)/shard_map/ppermute | solution.py:41
  180.4 17.1 %all-to-all-start.1 = ((f32[8,1,512]{2,1,0:T(1,128)}), f32[8,1,512]{2,1,0:T(1,128)S(1)}, u32[]{:S(2)}, u32[]{:S(2)}) async-start(f32[8,1,512]{2,1,0:T(1,128)} %broadcast_in_dim.46), calls=%async_computation.1 | async-start | bytes 32768 | tf_op jit(solution)/shard_map/all_to_all | solution.py:22
Sparse Core Ops, SparseCore 0:
  20.0 102.0 all-gather.4
where the time goes:
time: 247 us; the launch traced here: 246 us
  blocking collectives  96.8 us (39%)
  waiting for transfers between devices  36.6 us (15%)
  starting transfers between devices  26.3 us (11%)
  matrix products  25.9 us (10%)
  local copies, waits for them, and re-layouts  25.3 us (10%)
  other arithmetic  20.7 us (8%)
  between operations  14.1 us (6%)
    all_to_all x1, blocking collectives, sum_at_owner(): lax.all_to_all(in_blocks(value, dim, length), axis, 0, 0, tiled=True)  30.4 us
    all_gather x1, blocking collectives, shards(): totals = lax.all_gather(device_total[None], 'sp', axis=0, tiled=True)  28.2 us
    all_gather x1, blocking collectives, shards(): piece = lax.all_gather(local_final[None], 'sp', axis=0, tiled=True)  25.9 us
    all_to_all x2, waiting for transfers between devices, from_everyone(): lax.all_to_all(jnp.broadcast_to(value[None], (length, *value.shape)), axi...  24.1 us
    all_to_all x2, starting transfers between devices, from_everyone(): lax.all_to_all(jnp.broadcast_to(value[None], (length, *value.shape)), axi...  24 us
    all_gather x1, waiting for transfers between devices, side_by_side(): lax.all_gather(both, axis, axis=dim, tiled=True)  12.5 us
    all_gather x1, blocking collectives, side_by_side(): lax.all_gather(both, axis, axis=dim, tiled=True)  12.3 us
    unnamed x76, local copies, waits for them, and re-layouts  12.3 us
  transfers between devices with their start and end apart: 4, of which 3 were waited for; matrix products, arithmetic and copies ran while one was open for 13% of the time, Pallas kernels for 0%

commit v1 on v0

--- a/solution.py
+++ b/solution.py
@@ -195,7 +195,9 @@
     before = lax.dynamic_index_in_dim(
         running_totals, sp_index, 0, False
     ) - lax.dynamic_index_in_dim(totals, sp_index, 0, False)
-    piece = lax.all_gather(local_final[None], "sp", axis=0, tiled=True)
+    piece = jnp.concatenate(
+        lax.all_to_all(jnp.stack([local_final[None]] * lax.axis_size("sp")), "sp", 0, 0), axis=0
+    )
     number = piece.shape[0]
     anchor = jnp.arange(number, dtype=jnp.int32)
     exponent = jnp.where(

time: 247 us -> 238 us (0.964)
  blocking collectives: 96.8 us -> 75.9 us
  local copies, waits for them, and re-layouts: 25.3 us -> 31 us
  other arithmetic: 20.7 us -> 24.4 us
  matrix products: 25.9 us -> 28.6 us
  waiting for transfers between devices: 36.6 us -> 33.9 us
    all_gather x1 -> x0, blocking collectives: 25.9 us -> none  [shards(): piece = lax.all_gather(local_final[None], 'sp', axis=0, tiled=True)]
    all_to_all x0 -> x1, starting transfers between devices: none -> 10.2 us  [shards(): lax.all_to_all(jnp.stack([local_final[None]] * lax.axis_size('sp')), 'sp'...]
    all_to_all x2, starting transfers between devices: 24 us -> 17.2 us  [from_everyone(): lax.all_to_all(jnp.broadcast_to(value[None], (length, *value.shape)), axi...]
    all_to_all x1, blocking collectives: 30.4 us -> 35.4 us  [sum_at_owner(): lax.all_to_all(in_blocks(value, dim, length), axis, 0, 0, tiled=True)]
    all_to_all x2, waiting for transfers between devices: 24.1 us -> 20.5 us  [from_everyone(): lax.all_to_all(jnp.broadcast_to(value[None], (length, *value.shape)), axi...]
    unnamed x76 -> x24, local copies, waits for them, and re-layouts: 12.3 us -> 15.2 us
  transfers between devices with their start and end apart: 4 -> 5, of which waited for: 3 -> 3; matrix products, arithmetic and copies ran while one was open for 13% -> 24% of each run, Pallas kernels for 0% -> 0%
where the time goes in v1:
time: 238 us; the launch traced here: 236 us
  blocking collectives  75.9 us (32%)
  waiting for transfers between devices  33.9 us (14%)
  local copies, waits for them, and re-layouts  31 us (13%)
  starting transfers between devices  28.6 us (12%)
  matrix products  28.6 us (12%)
  other arithmetic  24.4 us (10%)
  between operations  13.7 us (6%)
    all_to_all x1, blocking collectives, sum_at_owner(): lax.all_to_all(in_blocks(value, dim, length), axis, 0, 0, tiled=True)  35.4 us
    all_gather x1, blocking collectives, shards(): totals = lax.all_gather(device_total[None], 'sp', axis=0, tiled=True)  28.2 us
    all_to_all x2, waiting for transfers between devices, from_everyone(): lax.all_to_all(jnp.broadcast_to(value[None], (length, *value.shape)), axi...  20.5 us
    all_to_all x2, starting transfers between devices, from_everyone(): lax.all_to_all(jnp.broadcast_to(value[None], (length, *value.shape)), axi...  17.2 us
    unnamed x24, local copies, waits for them, and re-layouts  15.2 us
    all_gather x1, blocking collectives, side_by_side(): lax.all_gather(both, axis, axis=dim, tiled=True)  12.3 us
    all_gather x1, waiting for transfers between devices, side_by_side(): lax.all_gather(both, axis, axis=dim, tiled=True)  12 us
    all_to_all x1, starting transfers between devices, shards(): lax.all_to_all(jnp.stack([local_final[None]] * lax.axis_size('sp')), 'sp'...  10.2 us
  transfers between devices with their start and end apart: 5, of which 3 were waited for; matrix products, arithmetic and copies ran while one was open for 24% of the time, Pallas kernels for 0%

profile of v1, /device:TPU:1, one launch (start us, length us, event | category | flops | bytes accessed | tf_op | source)
XLA Modules:
  0.0 236.2 jit_solution(380675715664380731)
XLA Ops:
  6.5 1.0 concatenate.11
  7.5 12.3 %all_gather.9 = bf16[256,896]{1,0:T(8,128)(2,1)} all-gather(bf16[64,896]{1,0:T(8,128)(2,1)S(1)} %concatenate.11), channel_id=1, replica_groups=mesh['sp'=16,'fs'=4,'tp'=8] {'fs'}, dimensions={0}, use_global_device_ids=true | all-gather | bytes 573440 | tf_op jit(solution)/shard_map/all_gather | solution.py:17
  19.8 1.1 copy.64
  20.9 1.5 broadcast_in_dim.39
  22.4 11.6 %all-to-all-start = ((bf16[8,256,512]{1,2,0:T(8,128)(2,1)}), bf16[8,256,512]{1,2,0:T(8,128)(2,1)S(1)}, u32[]{:S(2)}, u32[]{:S(2)}) async-start(bf16[8,256,512]{1,2,0:T(8,128)(2,1)} %broadcast_in_dim.39), calls=%async_computation | async-start | bytes 4194304 | tf_op jit(solution)/shard_map/all_to_all | solution.py:22
  34.0 0.8 dynamic_slice.30
  34.8 1.3 dynamic_slice.28
  36.2 1.7 dynamic-slice_bitcast_fusion.29
  37.8 2.0 fusion.98
  39.8 20.5 %all-to-all-done = bf16[8,256,512]{1,2,0:T(8,128)(2,1)S(1)} async-done(((bf16[8,256,512]{1,2,0:T(8,128)(2,1)}), bf16[8,256,512]{1,2,0:T(8,128)(2,1)S(1)}, u32[]{:S(2)}, u32[]{:S(2)}) %all-to-all-start) | async-done | bytes 2097184 | tf_op jit(solution)/shard_map/all_to_all | solution.py:22
  60.9 1.8 fusion.2
  62.7 2.2 fusion.86
  65.6 28.2 %all-gather.1 = f32[16,2,32]{2,1,0:T(2,128)S(1)} all-gather(f32[1,2,32]{2,1,0:T(2,128)S(1)} %bitcast.160), channel_id=2, replica_groups=mesh['sp'=16,'fs'=4,'tp'=8] {'sp'}, dimensions={0}, use_global_device_ids=true | all-gather | bytes 4352 | tf_op jit(solution)/shard_map/all_gather | solution.py:192
  94.0 4.5 %select_exponential_fusion = f32[4,2,64,64,32]{3,4,2,1,0:T(8,128)} fusion(f32[4,2,64,32]{2,3,1,0:T(8,128)S(1)} %copy.67, f32[4,2,64,32]{3,2,1,0:T(8,128)S(1)} %reduce_window_sum.35, pred[64,64]{1,0:T(8,128)(4,1)S(1)} %iota_compare_fusion), kind=kLoop, calls=%fused_computation.5 | loop fusion | flops 2097152 | bytes 4329472 | tf_op jit(solution)/shard_map/exp | solution.py:173
  98.5 11.0 %copy.82 = f32[4,2,64,64,32]{2,3,4,1,0:T(8,128)} copy(f32[4,2,64,64,32]{3,4,2,1,0:T(8,128)} %select_exponential_fusion) | data formatting | bytes 8388608
  110.1 12.0 %all-gather.4.cloned.1.call-done = bf16[4096,896]{1,0:T(8,128)(2,1)} async-done(((bf16[256,896]{1,0:T(8,128)(2,1)}), bf16[4096,896]{1,0:T(8,128)(2,1)}) %all-gather.4.cloned.1.call-update) | async-done | bytes 7340048 | tf_op jit(solution)/shard_map/all_gather | solution.py:17
  122.1 2.2 fusion.18
  124.4 0.8 copy.73
  125.3 2.0 fusion.13
  127.4 2.0 fusion.12
  129.4 2.0 fusion.6
  132.0 1.3 collective-permute-start
  133.3 1.0 fusion.38
  134.3 5.8 %while.13 = (s32[]{:T(128)}, f32[2,32,64]{2,1,0:T(8,128)S(1)}, f32[4,2,32,64]{3,2,1,0:T(8,128)}, f32[4,2,32]{2,1,0:T(2,128)S(1)}, f32[4,2,32,64]{3,2,1,0:T(8,128)}, /*index=5*/s32[]{:T(128)}, s32[]{:T(128)}) while((s32[]{:T(128)}, f32[2,32,64]{2,1,0:T(8,128)S(1)}, f32[4,2,32,64]{3,2,1,0:T(8,128)}, f32[4,2,32]{2,1,0:T(2,128)S(1)}, ...), condition=%wide.region_9.10_spmd.clone, body=%wide.region_8.9_spmd.clone.sunk | while | flops 16387 | bytes 99680 | solution.py:188
  134.9 0.8 bitcast_add_fusion.3
  136.4 0.8 bitcast_add_fusion.3
  137.8 0.8 bitcast_add_fusion.3
  139.3 0.8 bitcast_add_fusion.3
  140.2 2.0 fusion.101
  142.8 5.6 %all-to-all-start.1 = ((f32[8,1,512]{2,1,0:T(1,128)}), f32[8,1,512]{2,1,0:T(1,128)S(1)}, u32[]{:S(2)}, u32[]{:S(2)}) async-start(f32[8,1,512]{2,1,0:T(1,128)} %broadcast_in_dim.44), calls=%async_computation.1 | async-start | bytes 32768 | tf_op jit(solution)/shard_map/all_to_all | solution.py:22
  148.4 1.8 fusion.21
  150.1 0.9 stack.3
  151.0 2.1 reshape.98
  153.1 0.6 copy.68
  153.9 0.7 copy.69
  154.6 10.2 %all-to-all-start.2 = ((f32[16,1,4096]{2,1,0:T(1,128)}), f32[16,1,4096]{2,1,0:T(1,128)}, u32[]{:S(2)}, u32[]{:S(2)}) async-start(f32[16,1,4096]{2,1,0:T(1,128)} %reshape.98), calls=%async_computation.2 | async-start | bytes 524288 | tf_op jit(solution)/shard_map/all_to_all | solution.py:199
  164.7 6.0 %fusion = f32[4,2,64,64]{2,3,1,0:T(8,128)} fusion(f32[4,2,64,64,32]{2,3,4,1,0:T(8,128)} %copy.82, f32[4,2,32,64]{3,2,1,0:T(8,128)} %copy.69, f32[4,2,32,64]{3,2,1,0:T(8,128)} %copy.68), kind=kLoop, calls=%fused_computation.4 | loop fusion | flops 3112960 | bytes 4456448 | tf_op jit(solution)/shard_map/nhid,nhjd,nhijd->nhij/dot_general | solution.py:174
  170.8 0.9 copy.72
  171.6 2.0 fusion.73
  173.7 4.0 %fusion.31 = f32[4096,256]{1,0:T(8,128)} fusion(bf16[4096,896]{1,0:T(8,128)(2,1)} %all-gather.4.cloned.1.call-done, f32[256,128]{1,0:T(8,128)} %get-tuple-element.65, f32[128]{0:T(128)S(1)} %copy-done.9, f32[256]{0:T(256)S(1)} %get-tuple-element.100, f32[256]{0:T(256)S(1)} %get-tuple-element.99), kind=kOutput, calls=%fused_computation.50 | convolution fusion | flops 268697600 | bytes 5376512 | tf_op jit(solution)/shard_map/dot_general | solution.py:224
  177.6 1.5 all-to-all-done.2
  179.6 2.2 reduce.6
  181.9 1.0 reshape.99
  182.9 1.9 fusion.34
  184.8 1.8 multiply_reduce_fusion.1
  187.1 5.7 %fusion.1 = bf16[4096,256]{1,0:T(8,128)(2,1)} fusion(f32[4096,256]{1,0:T(8,128)} %fusion.31, bf16[4096,896]{1,0:T(8,128)(2,1)} %all-gather.4.cloned.1.call-done, f32[256,128]{1,0:T(8,128)S(1)} %reshape.84, bf16[256,4096]{0,1:T(8,128)(2,1)S(1)} %copy-done.1, f32[256]{0:T(256)S(1)} %copy-done.7), kind=kOutput, calls=%fused_computation.7 | convolution fusion | flops 539262976 | bytes 10617856 | tf_op jit(solution)/shard_map/dot_general | solution.py:230
  192.8 35.4 %all_to_all.21 = bf16[8,512,256]{2,1,0:T(8,128)(2,1)S(1)} all-to-all(bf16[8,512,256]{2,1,0:T(8,128)(2,1)} %bitcast.150), channel_id=1, replica_groups=mesh['sp'=16,'fs'=4,'tp'=8] {'tp'}, dimensions={0} | all-to-all | bytes 4194304 | tf_op jit(solution)/shard_map/all_to_all | solution.py:66
  228.5 0.8 copy.77
  (64 shorter events, 7.5 us)
Async XLA Ops:
  6.5 56.1 %copy-start = (bf16[4096,64]{0,1:T(8,128)(2,1)S(1)}, bf16[4096,64]{0,1:T(8,128)(2,1)}, u32[]{:S(2)}) copy-start(bf16[4096,64]{0,1:T(8,128)(2,1)} %param.29) | copy-start | bytes 1572868
  6.5 115.5 %all-gather.4.cloned.1.call-start = ((), (), s32[]{:S(2)}) async-start(), calls=%async_computation.4 | async-start | bytes 7798784 | tf_op jit(solution)/shard_map/all_gather | solution.py:17
  20.9 39.9 %copy-start.4 = (f32[4096]{0:T(1024)S(1)}, f32[4096]{0:T(1024)}, u32[]{:S(2)}) copy-start(f32[4096]{0:T(1024)} %param.20) | copy-start | bytes 49156
  22.4 37.8 %all-to-all-start = ((bf16[8,256,512]{1,2,0:T(8,128)(2,1)}), bf16[8,256,512]{1,2,0:T(8,128)(2,1)S(1)}, u32[]{:S(2)}, u32[]{:S(2)}) async-start(bf16[8,256,512]{1,2,0:T(8,128)(2,1)} %broadcast_in_dim.39), calls=%async_computation | async-start | bytes 4194304 | tf_op jit(solution)/shard_map/all_to_all | solution.py:22
  34.0 28.6 %copy-start.3 = (f32[1,256,64]{1,2,0:T(8,128)S(1)}, f32[1,256,64]{1,2,0:T(8,128)}, u32[]{:S(2)}) copy-start(f32[1,256,64]{1,2,0:T(8,128)} %param.32) | copy-start | bytes 196612
  60.9 68.5 %copy-start.6 = (f32[256]{0:T(256)}, f32[256]{0:T(256)S(1)}, u32[]{:S(2)}) copy-start(f32[256]{0:T(256)S(1)} %add_rsqrt_fusion.1) | copy-start | bytes 3076
  98.5 23.6 %copy-start.1 = (bf16[256,4096]{0,1:T(8,128)(2,1)S(1)}, bf16[256,4096]{0,1:T(8,128)(2,1)}, u32[]{:S(2)}) copy-start(bf16[256,4096]{0,1:T(8,128)(2,1)} %fusion.2) | copy-start | bytes 6291460
  127.4 5.9 %copy-start.2 = (f32[4,64,2,32]{3,1,2,0:T(8,128)S(1)}, f32[4,64,2,32]{3,1,2,0:T(8,128)}, u32[]{:S(2)}) copy-start(f32[4,64,2,32]{3,1,2,0:T(8,128)} %copy.73) | copy-start | bytes 196612
  132.0 8.2 %collective-permute-start = (bf16[30,128]{1,0:T(8,128)(2,1)}, bf16[30,128]{1,0:T(8,128)(2,1)S(1)}, u32[]{:S(2)}, u32[]{:S(2)}) collective-permute-start(bf16[30,128]{1,0:T(8,128)(2,1)} %slice.265), channel_id=1, source_target_pairs={{0,32},{32,64},{64,96},{96,128},{128,160},{160,192},{192,224},{224... | collective-permute-start | bytes 23048 | tf_op jit(solution)/shard_map/ppermute | solution.py:41
  142.8 11.8 %all-to-all-start.1 = ((f32[8,1,512]{2,1,0:T(1,128)}), f32[8,1,512]{2,1,0:T(1,128)S(1)}, u32[]{:S(2)}, u32[]{:S(2)}) async-start(f32[8,1,512]{2,1,0:T(1,128)} %broadcast_in_dim.44), calls=%async_computation.1 | async-start | bytes 32768 | tf_op jit(solution)/shard_map/all_to_all | solution.py:22
  154.6 24.6 %all-to-all-start.2 = ((f32[16,1,4096]{2,1,0:T(1,128)}), f32[16,1,4096]{2,1,0:T(1,128)}, u32[]{:S(2)}, u32[]{:S(2)}) async-start(f32[16,1,4096]{2,1,0:T(1,128)} %reshape.98), calls=%async_computation.2 | async-start | bytes 524288 | tf_op jit(solution)/shard_map/all_to_all | solution.py:199
  164.7 8.9 %copy-start.9 = (f32[128]{0:T(128)S(1)}, f32[128]{0:T(128)}, u32[]{:S(2)}) copy-start(f32[128]{0:T(128)} %dynamic_slice.28) | copy-start | bytes 1540
  170.7 14.0 %copy-start.5 = (f32[4,2,32]{2,1,0:T(2,128)S(1)}, f32[4,2,32]{2,1,0:T(2,128)}, u32[]{:S(2)}) copy-start(f32[4,2,32]{2,1,0:T(2,128)} %fusion.23) | copy-start | bytes 3076
  173.6 13.0 %copy-start.8 = (f32[64]{0:T(128)S(1)}, f32[64]{0:T(128)}, u32[]{:S(2)}) copy-start(f32[64]{0:T(128)} %param.35) | copy-start | bytes 772
  173.6 13.5 %copy-start.7 = (f32[256]{0:T(256)S(1)}, f32[256]{0:T(256)}, u32[]{:S(2)}) copy-start(f32[256]{0:T(256)} %copy-done.6) | copy-start | bytes 3076
Sparse Core Ops, SparseCore 0:
  20.0 102.0 all-gather.3
